TPU v7x, 512 devices: a whole 4x8x8 slice. The times are simulated.
512 devices in a mesh: ep: 32 (over z, x), tp: 16 (over y, core).
Axes of the slice: x: 4, y: 8, z: 8, core: 2. Of those that a mesh axis runs over, the one named last changes fastest.
Arguments:
- tokens: bfloat16 [768, 4096], P('ep'), may hold values from -6 to 6
- norm_gain: float32 [4096], replicated, may hold values from 0.1 to 1.9
- routes: int32 [768, 6], P('ep'), may hold values from 0 to 63, all different within a row; in each aligned block of 24 rows (0 to 23, 24 to 47, ...) at most 6 rows name the same one
- route_scores: float32 [768, 6], P('ep'), may hold values from 0.05 to 1
- expert_gate: bfloat16 [64, 1024, 4096], P('ep', 'tp'), may hold values from -0.09375 to 0.09375
- expert_up: bfloat16 [64, 1024, 4096], P('ep', 'tp'), may hold values from -0.09375 to 0.09375
- expert_down: bfloat16 [64, 1024, 4096], P('ep', 'tp'), may hold values from -0.1875 to 0.1875
- shared_gate: bfloat16 [1024, 4096], P('tp'), may hold values from -0.09375 to 0.09375
- shared_up: bfloat16 [1024, 4096], P('tp'), may hold values from -0.09375 to 0.09375
- shared_down: bfloat16 [1024, 4096], P('tp'), may hold values from -0.1875 to 0.1875
Outputs:
- mixed: bfloat16 [768, 4096], P('ep', 'tp')
Inputs may be any that keep to these rules, and one draw needn't show every extreme that they name: `routes`: each row names 6 different experts. In the rows of one device (aligned blocks of 24 rows) no expert is named by more than 6 rows, and in some block one expert is named by exactly 6 rows.
All inputs are finite; a program needn't handle non-finite values.
Results may differ from a plain program's by a relative error of at most 0.02.
Values may be sent and summed in bfloat16 or wider, within the bound.
No kernel may reach another device: no remote copies, remote signals or barrier semaphores. Data moves between devices by JAX's collectives and lax.ppermute only.
A program may use at most 64 MiB of HBM per device.

v0:
```python
import jax
import jax.numpy as jnp
from jax import lax
from jax.experimental import pallas as pl
from jax.experimental.pallas import tpu as pltpu
from jax.sharding import Mesh, PartitionSpec as P


NZ, NX, NY, NC = 8, 4, 8, 2
EP = NZ * NX
D = 4096
FF_DEV = 64
TOK = 24
TOPK = 6
EXPERTS = 64
CAP = 6
QUARTERS = 4
QW = D // QUARTERS
PIECE = CAP * QUARTERS
ROWS = EP * PIECE
SLOTS = EP * CAP
OUT_W = D // NY
HALF = OUT_W // NC
LANES = 128
GROUP = 32
NGROUPS = SLOTS // GROUP
MSG = NC * FF_DEV + TOK
ORDER = (0, 4, 5, 3, 6, 2, 7, 1)
BATCH = 8
PARTS = EP // BATCH
BACK = 16
BACK_ROWS = EXPERTS * BACK
VM = pl.BlockSpec(memory_space=pltpu.VMEM)
HB = pl.BlockSpec(memory_space=pltpu.HBM)
F32, BF16 = jnp.float32, jnp.bfloat16


def iota(shape, dim):
    return lax.broadcasted_iota(jnp.int32, shape, dim)


def nt(a, b):
    return lax.dot_general(a, b, (((1,), (1,)), ((), ())), preferred_element_type=F32)


def nn(a, b):
    return jnp.dot(a, b, preferred_element_type=F32)


def spread_tokens(values):
    lane, token = iota((TOK, LANES), 1), iota((TOK, LANES), 0)
    place = ((lane & (GROUP - 1)) == token).astype(F32).astype(BF16)
    return nn(values.astype(BF16), place)


def membership(routes, base):
    named = jnp.zeros((EXPERTS, TOK), F32)
    for k in range(TOPK):
        named += (routes[k : k + 1, :] == iota((EXPERTS, TOK), 0)).astype(F32)
    earlier = (iota((TOK, TOK), 0) < iota((TOK, TOK), 1)).astype(F32)
    rank = nn(named.astype(BF16), earlier.astype(BF16))
    return named * (rank + 1.0 + (base * (iota((EXPERTS, TOK), 0) >> 1)).astype(F32))


def pack_kernel(
    tok_hbm, gain_hbm, routes_hbm, send_ref, normed_ref, stack_ref, tok_ref, gain_ref, routes_ref, sems
):
    core = lax.axis_index("c")
    routes_copy = pltpu.make_async_copy(routes_hbm, routes_ref, sems.at[2])
    tok_copy = pltpu.make_async_copy(tok_hbm, tok_ref, sems.at[0])
    gain_copy = pltpu.make_async_copy(gain_hbm, gain_ref, sems.at[1])
    routes_copy.start()
    tok_copy.start()
    gain_copy.start()
    routes_copy.wait()
    code = spread_tokens(membership(routes_ref[...], CAP)).astype(BF16)
    row, expert = iota((ROWS, EXPERTS), 0), iota((ROWS, EXPERTS), 1)
    low = (expert - core) * (PIECE // 2)
    owner = ((expert & 1) == core) & (row >= low) & (row < low + PIECE)
    found = nn(owner.astype(F32).astype(BF16), code)
    row, col = iota((ROWS, LANES), 0), iota((ROWS, LANES), 1)
    table = (found == ((row >> 2) + 1).astype(F32)) & ((row & 3) == (col >> 5))
    table = table.astype(F32).astype(BF16)
    stack_ref[...] = jnp.zeros(stack_ref.shape, BF16)
    tok_copy.wait()
    gain_copy.wait()
    values = tok_ref[...].astype(F32)
    normed = (
        values * lax.rsqrt(jnp.mean(values * values, -1, keepdims=True) + 1e-06) * gain_ref[...]
    ).astype(BF16)
    normed_ref[...] = normed
    for q in range(QUARTERS):
        stack_ref[q * GROUP : q * GROUP + TOK, :] = normed[:, q * QW : (q + 1) * QW]
    chunk = ROWS // 4
    for k in range(4):
        send_ref[k * chunk : (k + 1) * chunk, :] = nn(
            table[k * chunk : (k + 1) * chunk, :], stack_ref[...]
        ).astype(BF16)


def side_kernel(normed_ref, sg_ref, su_ref, sd_ref, down_ref, *refs):
    messages, part_ref = refs[:NY], refs[NY]
    me = lax.axis_index("y")
    normed = normed_ref[...]
    gate, upper = nt(normed, sg_ref[...]), nt(normed, su_ref[...])
    hidden = (gate / (1.0 + jnp.exp(-gate)) * upper).astype(BF16)
    part_ref[...] = nn(hidden, sd_ref[...]).astype(BF16)
    for d in range(NY):
        cols = pl.ds(pl.multiple_of(lax.rem(me + d, NY) * OUT_W, OUT_W), OUT_W)
        messages[d][0:FF_DEV, :] = down_ref[0, :, cols]
        messages[d][FF_DEV : 2 * FF_DEV, :] = down_ref[1, :, cols]
        messages[d][2 * FF_DEV : MSG, :] = part_ref[:, cols]


def ready_kernel(*refs):
    messages, (keep_ref, give_ref, mine_ref, other_ref) = dict(zip(ORDER, refs)), refs[NY:]
    core, me = lax.axis_index("c"), lax.axis_index("y")
    shared = jnp.zeros((TOK, OUT_W), F32)
    for d in range(NY):
        source = lax.rem(me + NY - d, NY)
        rows = pl.ds(pl.multiple_of(source * FF_DEV, FF_DEV), FF_DEV)
        keep_ref[rows, :] = messages[d][pl.ds(pl.multiple_of(core * FF_DEV, FF_DEV), FF_DEV), :]
        give_ref[rows, :] = messages[d][
            pl.ds(pl.multiple_of((1 - core) * FF_DEV, FF_DEV), FF_DEV), :
        ]
        shared += messages[d][2 * FF_DEV : MSG, :].astype(F32)
    for half in range(NC):

        @pl.when(core == half)
        def _():
            mine_ref[...] = shared[:, half * HALF : (half + 1) * HALF]

        @pl.when(core != half)
        def _():
            other_ref[...] = shared[:, half * HALF : (half + 1) * HALF]


def hidden_kernel(
    rows_hbm,
    gate_hbm,
    got_gate_hbm,
    up_hbm,
    got_up_hbm,
    after_ref,
    out_ref,
    rows_ref,
    x_ref,
    weight_ref,
    row_sems,
    sems,
):
    core = lax.axis_index("c")
    pieces = [
        pltpu.make_async_copy(
            rows_hbm.at[g * LANES : (g + 1) * LANES, :],
            rows_ref.at[g * LANES : (g + 1) * LANES, :],
            row_sems.at[g],
        )
        for g in range(NGROUPS)
    ]
    copies = [
        pltpu.make_async_copy(
            ref.at[core], weight_ref.at[k * FF_DEV : (k + 1) * FF_DEV, :], sems.at[k]
        )
        for k, ref in enumerate((gate_hbm, got_gate_hbm, up_hbm, got_up_hbm))
    ]
    for copy in pieces + copies:
        copy.start()
    i, j = iota((LANES, LANES), 0), iota((LANES, LANES), 1)
    sort = (j == (i & (GROUP - 1)) * QUARTERS + (i >> 5)).astype(F32).astype(BF16)
    for g in range(NGROUPS):
        pieces[g].wait()
        block = nn(sort, rows_ref[g * LANES : (g + 1) * LANES, :]).astype(BF16)
        for q in range(QUARTERS):
            x_ref[g * GROUP : (g + 1) * GROUP, q * QW : (q + 1) * QW] = block[
                q * GROUP : (q + 1) * GROUP, :
            ]
    for copy in copies:
        copy.wait()
    both = nt(x_ref[...], weight_ref[...])
    gate, upper = both[:, : 2 * FF_DEV], both[:, 2 * FF_DEV :]
    hidden = (gate / (1.0 + jnp.exp(-gate)) * upper).astype(BF16)
    for d in range(NY):
        out_ref[d] = hidden


def weigh_kernel(routes_ref, scores_ref, chi_ref, clo_ref):
    routes, scores = routes_ref[...], scores_ref[...]
    weights = scores / jnp.sum(scores, 0, keepdims=True) * 2.5
    weight = jnp.zeros((EXPERTS, TOK), F32)
    for k in range(TOPK):
        weight += jnp.where(
            routes[k : k + 1, :] == iota((EXPERTS, TOK), 0), weights[k : k + 1, :], 0.0
        )
    high = weight.astype(BF16)
    rest = weight - high.astype(F32)
    rank = membership(routes, 0)
    half = NC * GROUP
    code = spread_tokens(rank).T[:half].astype(BF16)
    high = spread_tokens(high).T[:half].astype(BF16)
    rest = spread_tokens(rest).T[:half].astype(BF16)
    shape = (EXPERTS, BACK_ROWS)
    owner = ((iota(shape, 1) >> 4) == iota(shape, 0)).astype(F32).astype(BF16)
    found = nn(code, owner)
    token, row = iota((half, BACK_ROWS), 0), iota((half, BACK_ROWS), 1)
    table = (found == (((row >> 1) & 7) + 1).astype(F32)) & ((row & 1) == (token >> 5))
    chi_ref[...] = jnp.where(table, nn(high, owner), 0.0).astype(BF16)
    clo_ref[...] = jnp.where(table, nn(rest, owner), 0.0).astype(BF16)


def down_kernel(hidden_ref, keep_ref, got_ref, out_ref, h_ref, stack_ref):
    for d in range(NY):
        h_ref[:, d * FF_DEV : (d + 1) * FF_DEV] = hidden_ref[d, :, :FF_DEV]
        h_ref[:, (NY + d) * FF_DEV : (NY + d + 1) * FF_DEV] = hidden_ref[d, :, FF_DEV:]
    wide = NY * FF_DEV
    done = (nn(h_ref[:, :wide], keep_ref[...]) + nn(h_ref[:, wide:], got_ref[...])).astype(BF16)
    slots = BATCH * CAP
    for p in range(PARTS):
        for q in range(QUARTERS):
            stack_ref[(p * QUARTERS + q) * slots : (p * QUARTERS + q + 1) * slots, :] = done[
                p * slots : (p + 1) * slots, q * LANES : (q + 1) * LANES
            ]
    shape = (BATCH * NC * BACK, QUARTERS * slots)
    i, j = iota(shape, 0), iota(shape, 1)
    slot = (i >> 1) & 7
    quarter = ((i >> 4) & 1) * 2 + (i & 1)
    place = (j == quarter * slots + (i >> 5) * CAP + slot) & (slot < CAP)
    place = place.astype(F32).astype(BF16)
    for p in range(PARTS):
        out_ref[p * shape[0] : (p + 1) * shape[0], :] = nn(
            place, stack_ref[p * shape[1] : (p + 1) * shape[1], :]
        ).astype(BF16)


def combine_kernel(rows_ref, chi_ref, clo_ref, mine_ref, got_ref, out_ref):
    total = nn(chi_ref[...], rows_ref[...]) + nn(clo_ref[...], rows_ref[...])
    for q in range(NC):
        cols = slice(q * LANES, (q + 1) * LANES)
        out_ref[:, cols] = (
            total[q * GROUP : q * GROUP + TOK, :] + (mine_ref[:, cols] + got_ref[:, cols])
        ).astype(BF16)


def call(kernel, outs, scratch, flops, *args, specs=None, grant=24):
    return pl.pallas_call(
        kernel,
        out_shape=outs,
        in_specs=specs or [VM] * len(args),
        out_specs=jax.tree.map(lambda _: VM, outs),
        scratch_shapes=scratch,
        compiler_params=pltpu.CompilerParams(vmem_limit_bytes=grant << 20),
        cost_estimate=pl.CostEstimate(flops=flops, bytes_accessed=1 << 20, transcendentals=0),
    )(*args)


def out(shape, dtype=BF16):
    return jax.ShapeDtypeStruct(shape, dtype)


def hop(x, axis, size, step):
    return lax.ppermute(x, axis, [(i, (i + step) % size) for i in range(size)])


def body(
    tokens,
    norm_gain,
    routes,
    route_scores,
    expert_gate,
    expert_up,
    expert_down,
    shared_gate,
    shared_up,
    shared_down,
):
    send, normed = call(
        pack_kernel,
        (out((ROWS, QW)), out((TOK, D))),
        [
            pltpu.VMEM((LANES, QW), BF16),
            pltpu.VMEM((TOK, D), BF16),
            pltpu.VMEM((1, D), F32),
            pltpu.VMEM((TOPK, TOK), jnp.int32),
            pltpu.SemaphoreType.DMA((3,)),
        ],
        1 << 30,
        tokens,
        norm_gain.reshape(1, D),
        routes.T,
        specs=[HB] * 3,
        grant=62,
    )
    rows = lax.all_to_all(
        send.reshape(EP, PIECE, QW), ("z", "x"), split_axis=0, concat_axis=0, tiled=True
    ).reshape(ROWS, QW)
    messages = list(
        call(
            side_kernel,
            tuple(out((MSG, OUT_W)) for _ in range(NY)),
            [pltpu.VMEM((TOK, D), BF16)],
            1 << 30,
            normed,
            shared_gate,
            shared_up,
            shared_down,
            expert_down,
        )
    )
    for d in ORDER[1:]:
        messages[d] = hop(messages[d], "y", NY, d)
    got_gate = hop(expert_gate, "c", NC, 1)
    got_up = hop(expert_up, "c", NC, 1)
    chi, clo = call(
        weigh_kernel,
        (out((NC * GROUP, BACK_ROWS)), out((NC * GROUP, BACK_ROWS))),
        [],
        1 << 28,
        routes.T,
        route_scores.T,
    )
    wide = NY * FF_DEV
    keep, give, mine, other = call(
        ready_kernel,
        (out((wide, OUT_W)), out((wide, OUT_W)), out((TOK, HALF), F32), out((TOK, HALF), F32)),
        [],
        1 << 28,
        *[messages[d] for d in ORDER],
    )
    got, other = hop(give, "c", NC, 1), hop(other, "c", NC, 1)
    hidden = call(
        hidden_kernel,
        out((NY, SLOTS, 2 * FF_DEV)),
        [
            pltpu.VMEM((ROWS, QW), BF16),
            pltpu.VMEM((SLOTS, D), BF16),
            pltpu.VMEM((4 * FF_DEV, D), BF16),
            pltpu.SemaphoreType.DMA((NGROUPS,)),
            pltpu.SemaphoreType.DMA((4,)),
        ],
        1 << 30,
        rows,
        expert_gate,
        got_gate,
        expert_up,
        got_up,
        mine,
        specs=[HB] * 5 + [VM],
        grant=60,
    )
    hidden = lax.all_to_all(hidden, "y", split_axis=0, concat_axis=0, tiled=True)
    back = call(
        down_kernel,
        out((BACK_ROWS, LANES)),
        [pltpu.VMEM((SLOTS, 2 * wide), BF16), pltpu.VMEM((QUARTERS * SLOTS, LANES), BF16)],
        1 << 30,
        hidden,
        keep,
        got,
    )
    back = lax.all_to_all(
        back.reshape(EXPERTS, BACK, LANES), ("z", "x", "c"), split_axis=0, concat_axis=0, tiled=True
    ).reshape(BACK_ROWS, LANES)
    return call(combine_kernel, out((TOK, HALF)), [], 1 << 28, back, chi, clo, mine, other)


def solution(mesh):
    fine = Mesh(mesh.devices.reshape(NZ, NX, NY, NC), ("z", "x", "y", "c"))
    ep, tp = ("z", "x"), ("y", "c")
    in_specs = (
        P(ep, None),
        P(),
        P(ep, None),
        P(ep, None),
        P(ep, tp, None),
        P(ep, tp, None),
        P(ep, tp, None),
        P(tp, None),
        P(tp, None),
        P(tp, None),
    )
    return jax.shard_map(body, mesh=fine, in_specs=in_specs, out_specs=P(ep, tp), check_vma=False)
```

profile of v0, /device:TPU:1, one launch (start us, length us, event | category | flops | bytes accessed | tf_op | source)
XLA Modules:
  0.0 114.6 jit_solution(4114108374662486830)
XLA Ops:
  0.0 3.1 %shard_map.100 = (bf16[768,1024]{1,0:T(8,128)(2,1)}, bf16[24,4096]{1,0:T(8,128)(2,1)}) custom-call(bf16[24,4096]{1,0:T(8,128)(2,1)} %tok_hbm.1, f32[1,4096]{1,0:T(1,128)} %bitcast.12, s32[6,24]{1,0:T(8,128)} %bitcast.8), custom_call_target="tpu_custom_call" | custom-call | flops 1073741824 | bytes 1048576 | tf_op jit(solution)/shard_map/pallas_call | solution.py:245
  3.1 0.0 copy-start.2
  3.1 0.0 copy-start.3
  3.1 0.0 copy-start.4
  3.1 0.0 copy-start.5
  3.2 0.0 copy-start.8
  3.2 14.1 %all-to-all-start = ((bf16[32,24,1024]{2,1,0:T(8,128)(2,1)}), bf16[32,24,1024]{2,1,0:T(8,128)(2,1)}, u32[]{:S(2)}, u32[]{:S(2)}) async-start(bf16[32,24,1024]{2,1,0:T(8,128)(2,1)} %bitcast.11), calls=%async_computation | async-start | bytes 3145728 | tf_op jit(solution)/shard_map/all_to_all | solution.py:293
  17.3 2.9 %collective-permute-start = (bf16[2,64,4096]{2,1,0:T(8,128)(2,1)}, bf16[2,64,4096]{2,1,0:T(8,128)(2,1)}, u32[]{:S(2)}, u32[]{:S(2)}) collective-permute-start(bf16[2,64,4096]{2,1,0:T(8,128)(2,1)} %gate_hbm.1), channel_id=1, source_target_pairs={{0,1},{1,0},{2,3},{3,2},{4,5},{5,4},{6,7},{7,6},{8,9},{9,8},{10,11... | collective-permute-start | bytes 3145736 | tf_op jit(solution)/shard_map/ppermute | solution.py:261
  20.1 1.9 %collective-permute-start.1 = (bf16[2,64,4096]{2,1,0:T(8,128)(2,1)}, bf16[2,64,4096]{2,1,0:T(8,128)(2,1)}, u32[]{:S(2)}, u32[]{:S(2)}) collective-permute-start(bf16[2,64,4096]{2,1,0:T(8,128)(2,1)} %up_hbm.1), channel_id=1, source_target_pairs={{0,1},{1,0},{2,3},{3,2},{4,5},{5,4},{6,7},{7,6},{8,9},{9,8},{10,11... | collective-permute-start | bytes 3145736 | tf_op jit(solution)/shard_map/ppermute | solution.py:261
  22.1 0.0 copy-done.2
  22.1 0.0 copy-done.3
  22.1 0.0 copy-done.4
  22.1 0.0 copy-done.5
  22.1 0.0 copy-done.8
  22.1 0.6 shard_map.101
  22.8 7.5 %collective-permute-start.2 = (bf16[152,512]{1,0:T(8,128)(2,1)S(1)}, bf16[152,512]{1,0:T(8,128)(2,1)S(1)}, u32[]{:S(2)}, u32[]{:S(2)}) collective-permute-start(bf16[152,512]{1,0:T(8,128)(2,1)S(1)} %get-tuple-element.24), channel_id=1, source_target_pairs={{0,8},{2,10},{4,12},{6,14},{8,0},{10,2},{12,4},{14,6},{1,9},{3,11}... | collective-permute-start | bytes 466952 | tf_op jit(solution)/shard_map/ppermute | solution.py:261
  30.2 1.9 %collective-permute-start.3 = (bf16[152,512]{1,0:T(8,128)(2,1)S(1)}, bf16[152,512]{1,0:T(8,128)(2,1)S(1)}, u32[]{:S(2)}, u32[]{:S(2)}) collective-permute-start(bf16[152,512]{1,0:T(8,128)(2,1)S(1)} %get-tuple-element.25), channel_id=1, source_target_pairs={{0,10},{2,12},{4,14},{6,0},{8,2},{10,4},{12,6},{14,8},{1,11},{3,13... | collective-permute-start | bytes 466952 | tf_op jit(solution)/shard_map/ppermute | solution.py:261
  32.1 5.2 %collective-permute-start.4 = (bf16[152,512]{1,0:T(8,128)(2,1)S(1)}, bf16[152,512]{1,0:T(8,128)(2,1)S(1)}, u32[]{:S(2)}, u32[]{:S(2)}) collective-permute-start(bf16[152,512]{1,0:T(8,128)(2,1)S(1)} %get-tuple-element.26), channel_id=1, source_target_pairs={{0,6},{2,8},{4,10},{6,12},{8,14},{10,0},{12,2},{14,4},{1,7},{3,9},... | collective-permute-start | bytes 466952 | tf_op jit(solution)/shard_map/ppermute | solution.py:261
  37.3 0.0 collective-permute-done.2.refs_1_
  37.3 5.5 %collective-permute-start.5 = (bf16[152,512]{1,0:T(8,128)(2,1)S(1)}, bf16[152,512]{1,0:T(8,128)(2,1)S(1)}, u32[]{:S(2)}, u32[]{:S(2)}) collective-permute-start(bf16[152,512]{1,0:T(8,128)(2,1)S(1)} %get-tuple-element.27), channel_id=1, source_target_pairs={{0,12},{2,14},{4,0},{6,2},{8,4},{10,6},{12,8},{14,10},{1,13},{3,15... | collective-permute-start | bytes 466952 | tf_op jit(solution)/shard_map/ppermute | solution.py:261
  42.8 4.8 %collective-permute-done.3.refs_2_ = bf16[152,512]{1,0:T(8,128)(2,1)S(1)} collective-permute-done((bf16[152,512]{1,0:T(8,128)(2,1)S(1)}, bf16[152,512]{1,0:T(8,128)(2,1)S(1)}, u32[]{:S(2)}, u32[]{:S(2)}) %collective-permute-start.3) | collective-permute-done | bytes 155680 | tf_op jit(solution)/shard_map/ppermute | solution.py:261
  47.6 2.9 %collective-permute-start.6 = (bf16[152,512]{1,0:T(8,128)(2,1)S(1)}, bf16[152,512]{1,0:T(8,128)(2,1)S(1)}, u32[]{:S(2)}, u32[]{:S(2)}) collective-permute-start(bf16[152,512]{1,0:T(8,128)(2,1)S(1)} %get-tuple-element.28), channel_id=1, source_target_pairs={{0,4},{2,6},{4,8},{6,10},{8,12},{10,14},{12,0},{14,2},{1,5},{3,7},... | collective-permute-start | bytes 466952 | tf_op jit(solution)/shard_map/ppermute | solution.py:261
  50.6 0.0 collective-permute-done.4.refs_3_
  50.6 5.3 %collective-permute-start.7 = (bf16[152,512]{1,0:T(8,128)(2,1)S(1)}, bf16[152,512]{1,0:T(8,128)(2,1)S(1)}, u32[]{:S(2)}, u32[]{:S(2)}) collective-permute-start(bf16[152,512]{1,0:T(8,128)(2,1)S(1)} %get-tuple-element.29), channel_id=1, source_target_pairs={{0,14},{2,0},{4,2},{6,4},{8,6},{10,8},{12,10},{14,12},{1,15},{3,1}... | collective-permute-start | bytes 466952 | tf_op jit(solution)/shard_map/ppermute | solution.py:261
  55.9 0.0 collective-permute-done.5.refs_4_
  55.9 1.9 %collective-permute-start.8 = (bf16[152,512]{1,0:T(8,128)(2,1)S(1)}, bf16[152,512]{1,0:T(8,128)(2,1)S(1)}, u32[]{:S(2)}, u32[]{:S(2)}) collective-permute-start(bf16[152,512]{1,0:T(8,128)(2,1)S(1)} %get-tuple-element.30), channel_id=1, source_target_pairs={{0,2},{2,4},{4,6},{6,8},{8,10},{10,12},{12,14},{14,0},{1,3},{3,5},... | collective-permute-start | bytes 466952 | tf_op jit(solution)/shard_map/ppermute | solution.py:261
  57.8 0.0 collective-permute-done.6.refs_5_
  57.8 0.9 collective-permute-done.7.refs_6_
  58.8 5.1 %collective-permute-done.8.refs_7_ = bf16[152,512]{1,0:T(8,128)(2,1)S(1)} collective-permute-done((bf16[152,512]{1,0:T(8,128)(2,1)S(1)}, bf16[152,512]{1,0:T(8,128)(2,1)S(1)}, u32[]{:S(2)}, u32[]{:S(2)}) %collective-permute-start.8) | collective-permute-done | bytes 155680 | tf_op jit(solution)/shard_map/ppermute | solution.py:261
  63.8 0.1 shard_map.102
  64.0 0.0 copy-start
  64.0 0.6 copy-done
  64.6 0.0 collective-permute-done.got_gate_hbm
  64.6 0.0 collective-permute-done.1.got_up_hbm
  64.6 0.0 all-to-all-done
  64.6 4.7 %shard_map.103 = bf16[8,192,128]{2,1,0:T(8,128)(2,1)} custom-call(bf16[768,1024]{1,0:T(8,128)(2,1)} %bitcast.3.rows_hbm, bf16[2,64,4096]{2,1,0:T(8,128)(2,1)} %gate_hbm.1, bf16[2,64,4096]{2,1,0:T(8,128)(2,1)} %collective-permute-done.got_gate_hbm, bf16[2,64,4096]{2,1,0:T(8,128)(2,1)} %up_hbm.1, bf16[2,64,4096]{2,1,0:T(8,128)(2,1)} %collective-permute-done.1.got_up_hbm, ...), custom_call_target="tpu_custom_call" | custom-call | flops 1073741824 | bytes 1048576 | tf_op jit(solution)/shard_map/pallas_call | solution.py:245
  69.3 3.9 %all-to-all-start.1 = ((bf16[8,192,128]{2,1,0:T(8,128)(2,1)}), bf16[8,192,128]{2,1,0:T(8,128)(2,1)S(1)}, u32[]{:S(2)}, u32[]{:S(2)}) async-start(bf16[8,192,128]{2,1,0:T(8,128)(2,1)} %shard_map.103), calls=%async_computation.1 | async-start | bytes 786432 | tf_op jit(solution)/shard_map/all_to_all | solution.py:350
  73.2 4.7 %collective-permute-start.9 = (bf16[512,512]{1,0:T(8,128)(2,1)S(1)}, bf16[512,512]{1,0:T(8,128)(2,1)S(1)}, u32[]{:S(2)}, u32[]{:S(2)}) collective-permute-start(bf16[512,512]{1,0:T(8,128)(2,1)S(1)} %get-tuple-element.33), channel_id=1, source_target_pairs={{0,1},{1,0},{2,3},{3,2},{4,5},{5,4},{6,7},{7,6},{8,9},{9,8},{10,11... | collective-permute-start | bytes 1572872 | tf_op jit(solution)/shard_map/ppermute | solution.py:261
  77.8 1.5 %collective-permute-done.9.got_ref = bf16[512,512]{1,0:T(8,128)(2,1)S(1)} collective-permute-done((bf16[512,512]{1,0:T(8,128)(2,1)S(1)}, bf16[512,512]{1,0:T(8,128)(2,1)S(1)}, u32[]{:S(2)}, u32[]{:S(2)}) %collective-permute-start.9) | collective-permute-done | bytes 524320 | tf_op jit(solution)/shard_map/ppermute | solution.py:261
  79.4 5.4 %all-to-all-done.1.hidden_ref = bf16[8,192,128]{2,1,0:T(8,128)(2,1)S(1)} async-done(((bf16[8,192,128]{2,1,0:T(8,128)(2,1)}), bf16[8,192,128]{2,1,0:T(8,128)(2,1)S(1)}, u32[]{:S(2)}, u32[]{:S(2)}) %all-to-all-start.1) | async-done | bytes 393248 | tf_op jit(solution)/shard_map/all_to_all | solution.py:350
  84.7 1.5 %shard_map.104 = bf16[1024,128]{1,0:T(8,128)(2,1)} custom-call(bf16[8,192,128]{2,1,0:T(8,128)(2,1)S(1)} %all-to-all-done.1.hidden_ref, bf16[512,512]{1,0:T(8,128)(2,1)S(1)} %get-tuple-element.32.keep_ref, bf16[512,512]{1,0:T(8,128)(2,1)S(1)} %collective-permute-done.9.got_ref), custom_call_target="tpu_custom_call" | custom-call | flops 1073741824 | bytes 1048576 | tf_op jit(solution)/shard_map/pallas_call | solution.py:245
  86.2 14.5 %all-to-all-start.2 = ((bf16[64,16,128]{2,1,0:T(8,128)(2,1)}), bf16[64,16,128]{2,1,0:T(8,128)(2,1)S(1)}, u32[]{:S(2)}, u32[]{:S(2)}) async-start(bf16[64,16,128]{2,1,0:T(8,128)(2,1)} %bitcast.4), calls=%async_computation.2 | async-start | bytes 524288 | tf_op jit(solution)/shard_map/all_to_all | solution.py:360
  100.7 2.4 %collective-permute-start.10 = (f32[24,256]{1,0:T(8,128)S(1)}, f32[24,256]{1,0:T(8,128)S(1)}, u32[]{:S(2)}, u32[]{:S(2)}) collective-permute-start(f32[24,256]{1,0:T(8,128)S(1)} %get-tuple-element.36), channel_id=1, source_target_pairs={{0,1},{1,0},{2,3},{3,2},{4,5},{5,4},{6,7},{7,6},{8,9},{9,8},{10,11... | collective-permute-start | bytes 73736 | tf_op jit(solution)/shard_map/ppermute | solution.py:261
  103.0 0.6 shard_map.105
  103.6 0.2 collective-permute-done.10.got_ref
  103.9 9.9 %all-to-all-done.2 = bf16[64,16,128]{2,1,0:T(8,128)(2,1)S(1)} async-done(((bf16[64,16,128]{2,1,0:T(8,128)(2,1)}), bf16[64,16,128]{2,1,0:T(8,128)(2,1)S(1)}, u32[]{:S(2)}, u32[]{:S(2)}) %all-to-all-start.2) | async-done | bytes 262176 | tf_op jit(solution)/shard_map/all_to_all | solution.py:360
  113.7 0.0 copy-done.1
  113.7 0.8 shard_map.106
  (5 shorter events, 0.0 us)
Async XLA Ops:
  3.1 19.0 %copy-start.2 = (bf16[2,64,4096]{2,1,0:T(8,128)(2,1)S(1)}, bf16[2,64,4096]{2,1,0:T(8,128)(2,1)}, u32[]{:S(2)}) copy-start(bf16[2,64,4096]{2,1,0:T(8,128)(2,1)} %down_ref.1) | copy-start | bytes 3145732
  3.1 19.0 %copy-start.3 = (bf16[64,4096]{1,0:T(8,128)(2,1)S(1)}, bf16[64,4096]{1,0:T(8,128)(2,1)}, u32[]{:S(2)}) copy-start(bf16[64,4096]{1,0:T(8,128)(2,1)} %sg_ref.1) | copy-start | bytes 1572868
  3.1 19.0 %copy-start.4 = (bf16[64,4096]{1,0:T(8,128)(2,1)S(1)}, bf16[64,4096]{1,0:T(8,128)(2,1)}, u32[]{:S(2)}) copy-start(bf16[64,4096]{1,0:T(8,128)(2,1)} %su_ref.1) | copy-start | bytes 1572868
  3.1 19.0 %copy-start.5 = (bf16[64,4096]{1,0:T(8,128)(2,1)S(1)}, bf16[64,4096]{1,0:T(8,128)(2,1)}, u32[]{:S(2)}) copy-start(bf16[64,4096]{1,0:T(8,128)(2,1)} %sd_ref.1) | copy-start | bytes 1572868
  3.2 19.0 %copy-start.8 = (bf16[24,4096]{1,0:T(8,128)(2,1)S(1)}, bf16[24,4096]{1,0:T(8,128)(2,1)}, u32[]{:S(2)}) copy-start(bf16[24,4096]{1,0:T(8,128)(2,1)} %get-tuple-element.22.normed_ref) | copy-start | bytes 589828
  3.2 61.4 %all-to-all-start = ((bf16[32,24,1024]{2,1,0:T(8,128)(2,1)}), bf16[32,24,1024]{2,1,0:T(8,128)(2,1)}, u32[]{:S(2)}, u32[]{:S(2)}) async-start(bf16[32,24,1024]{2,1,0:T(8,128)(2,1)} %bitcast.11), calls=%async_computation | async-start | bytes 3145728 | tf_op jit(solution)/shard_map/all_to_all | solution.py:293
  17.3 47.3 %collective-permute-start = (bf16[2,64,4096]{2,1,0:T(8,128)(2,1)}, bf16[2,64,4096]{2,1,0:T(8,128)(2,1)}, u32[]{:S(2)}, u32[]{:S(2)}) collective-permute-start(bf16[2,64,4096]{2,1,0:T(8,128)(2,1)} %gate_hbm.1), channel_id=1, source_target_pairs={{0,1},{1,0},{2,3},{3,2},{4,5},{5,4},{6,7},{7,6},{8,9},{9,8},{10,11... | collective-permute-start | bytes 3145736 | tf_op jit(solution)/shard_map/ppermute | solution.py:261
  20.1 44.4 %collective-permute-start.1 = (bf16[2,64,4096]{2,1,0:T(8,128)(2,1)}, bf16[2,64,4096]{2,1,0:T(8,128)(2,1)}, u32[]{:S(2)}, u32[]{:S(2)}) collective-permute-start(bf16[2,64,4096]{2,1,0:T(8,128)(2,1)} %up_hbm.1), channel_id=1, source_target_pairs={{0,1},{1,0},{2,3},{3,2},{4,5},{5,4},{6,7},{7,6},{8,9},{9,8},{10,11... | collective-permute-start | bytes 3145736 | tf_op jit(solution)/shard_map/ppermute | solution.py:261
  22.8 14.6 %collective-permute-start.2 = (bf16[152,512]{1,0:T(8,128)(2,1)S(1)}, bf16[152,512]{1,0:T(8,128)(2,1)S(1)}, u32[]{:S(2)}, u32[]{:S(2)}) collective-permute-start(bf16[152,512]{1,0:T(8,128)(2,1)S(1)} %get-tuple-element.24), channel_id=1, source_target_pairs={{0,8},{2,10},{4,12},{6,14},{8,0},{10,2},{12,4},{14,6},{1,9},{3,11}... | collective-permute-start | bytes 466952 | tf_op jit(solution)/shard_map/ppermute | solution.py:261
  30.2 17.4 %collective-permute-start.3 = (bf16[152,512]{1,0:T(8,128)(2,1)S(1)}, bf16[152,512]{1,0:T(8,128)(2,1)S(1)}, u32[]{:S(2)}, u32[]{:S(2)}) collective-permute-start(bf16[152,512]{1,0:T(8,128)(2,1)S(1)} %get-tuple-element.25), channel_id=1, source_target_pairs={{0,10},{2,12},{4,14},{6,0},{8,2},{10,4},{12,6},{14,8},{1,11},{3,13... | collective-permute-start | bytes 466952 | tf_op jit(solution)/shard_map/ppermute | solution.py:261
  32.1 18.4 %collective-permute-start.4 = (bf16[152,512]{1,0:T(8,128)(2,1)S(1)}, bf16[152,512]{1,0:T(8,128)(2,1)S(1)}, u32[]{:S(2)}, u32[]{:S(2)}) collective-permute-start(bf16[152,512]{1,0:T(8,128)(2,1)S(1)} %get-tuple-element.26), channel_id=1, source_target_pairs={{0,6},{2,8},{4,10},{6,12},{8,14},{10,0},{12,2},{14,4},{1,7},{3,9},... | collective-permute-start | bytes 466952 | tf_op jit(solution)/shard_map/ppermute | solution.py:261
  37.3 18.5 %collective-permute-start.5 = (bf16[152,512]{1,0:T(8,128)(2,1)S(1)}, bf16[152,512]{1,0:T(8,128)(2,1)S(1)}, u32[]{:S(2)}, u32[]{:S(2)}) collective-permute-start(bf16[152,512]{1,0:T(8,128)(2,1)S(1)} %get-tuple-element.27), channel_id=1, source_target_pairs={{0,12},{2,14},{4,0},{6,2},{8,4},{10,6},{12,8},{14,10},{1,13},{3,15... | collective-permute-start | bytes 466952 | tf_op jit(solution)/shard_map/ppermute | solution.py:261
  47.6 10.2 %collective-permute-start.6 = (bf16[152,512]{1,0:T(8,128)(2,1)S(1)}, bf16[152,512]{1,0:T(8,128)(2,1)S(1)}, u32[]{:S(2)}, u32[]{:S(2)}) collective-permute-start(bf16[152,512]{1,0:T(8,128)(2,1)S(1)} %get-tuple-element.28), channel_id=1, source_target_pairs={{0,4},{2,6},{4,8},{6,10},{8,12},{10,14},{12,0},{14,2},{1,5},{3,7},... | collective-permute-start | bytes 466952 | tf_op jit(solution)/shard_map/ppermute | solution.py:261
  50.6 8.2 %collective-permute-start.7 = (bf16[152,512]{1,0:T(8,128)(2,1)S(1)}, bf16[152,512]{1,0:T(8,128)(2,1)S(1)}, u32[]{:S(2)}, u32[]{:S(2)}) collective-permute-start(bf16[152,512]{1,0:T(8,128)(2,1)S(1)} %get-tuple-element.29), channel_id=1, source_target_pairs={{0,14},{2,0},{4,2},{6,4},{8,6},{10,8},{12,10},{14,12},{1,15},{3,1}... | collective-permute-start | bytes 466952 | tf_op jit(solution)/shard_map/ppermute | solution.py:261
  55.9 7.9 %collective-permute-start.8 = (bf16[152,512]{1,0:T(8,128)(2,1)S(1)}, bf16[152,512]{1,0:T(8,128)(2,1)S(1)}, u32[]{:S(2)}, u32[]{:S(2)}) collective-permute-start(bf16[152,512]{1,0:T(8,128)(2,1)S(1)} %get-tuple-element.30), channel_id=1, source_target_pairs={{0,2},{2,4},{4,6},{6,8},{8,10},{10,12},{12,14},{14,0},{1,3},{3,5},... | collective-permute-start | bytes 466952 | tf_op jit(solution)/shard_map/ppermute | solution.py:261
  64.0 0.6 copy-start
  69.3 15.4 %all-to-all-start.1 = ((bf16[8,192,128]{2,1,0:T(8,128)(2,1)}), bf16[8,192,128]{2,1,0:T(8,128)(2,1)S(1)}, u32[]{:S(2)}, u32[]{:S(2)}) async-start(bf16[8,192,128]{2,1,0:T(8,128)(2,1)} %shard_map.103), calls=%async_computation.1 | async-start | bytes 786432 | tf_op jit(solution)/shard_map/all_to_all | solution.py:350
  73.2 6.2 %collective-permute-start.9 = (bf16[512,512]{1,0:T(8,128)(2,1)S(1)}, bf16[512,512]{1,0:T(8,128)(2,1)S(1)}, u32[]{:S(2)}, u32[]{:S(2)}) collective-permute-start(bf16[512,512]{1,0:T(8,128)(2,1)S(1)} %get-tuple-element.33), channel_id=1, source_target_pairs={{0,1},{1,0},{2,3},{3,2},{4,5},{5,4},{6,7},{7,6},{8,9},{9,8},{10,11... | collective-permute-start | bytes 1572872 | tf_op jit(solution)/shard_map/ppermute | solution.py:261
  84.7 18.3 %copy-start.6 = (s32[24,6]{0,1:T(8,128)S(1)}, s32[24,6]{0,1:T(8,128)}, u32[]{:S(2)}) copy-start(s32[24,6]{0,1:T(8,128)} %param.12) | copy-start | bytes 1732
  84.7 18.3 %copy-start.7 = (f32[24,6]{0,1:T(8,128)S(1)}, f32[24,6]{0,1:T(8,128)}, u32[]{:S(2)}) copy-start(f32[24,6]{0,1:T(8,128)} %param.13) | copy-start | bytes 1732
  84.7 29.0 %copy-start.1 = (f32[24,256]{1,0:T(8,128)S(1)}, f32[24,256]{1,0:T(8,128)}, u32[]{:S(2)}) copy-start(f32[24,256]{1,0:T(8,128)} %copy-done) | copy-start | bytes 73732
  86.2 27.5 %all-to-all-start.2 = ((bf16[64,16,128]{2,1,0:T(8,128)(2,1)}), bf16[64,16,128]{2,1,0:T(8,128)(2,1)S(1)}, u32[]{:S(2)}, u32[]{:S(2)}) async-start(bf16[64,16,128]{2,1,0:T(8,128)(2,1)} %bitcast.4), calls=%async_computation.2 | async-start | bytes 524288 | tf_op jit(solution)/shard_map/all_to_all | solution.py:360
  100.7 3.2 %collective-permute-start.10 = (f32[24,256]{1,0:T(8,128)S(1)}, f32[24,256]{1,0:T(8,128)S(1)}, u32[]{:S(2)}, u32[]{:S(2)}) collective-permute-start(f32[24,256]{1,0:T(8,128)S(1)} %get-tuple-element.36), channel_id=1, source_target_pairs={{0,1},{1,0},{2,3},{3,2},{4,5},{5,4},{6,7},{7,6},{8,9},{9,8},{10,11... | collective-permute-start | bytes 73736 | tf_op jit(solution)/shard_map/ppermute | solution.py:261
where the time goes:
time: 115 us
  starting transfers between devices  74.4 us (65%)
  waiting for transfers between devices  27.8 us (24%)
  Pallas kernels  11.4 us (10%)
    ppermute x11, starting transfers between devices, hop(): return lax.ppermute(x, axis, [(i, (i + step) % size) for i in range(size)])  42 us
    all_to_all x1, starting transfers between devices, body(): lax.all_to_all(back.reshape(EXPERTS, BACK, LANES), ('z', 'x', 'c'), split...  14.5 us
    all_to_all x1, starting transfers between devices, body(): lax.all_to_all(send.reshape(EP, PIECE, QW), ('z', 'x'), split_axis=0, con...  14.1 us
    ppermute x11, waiting for transfers between devices, hop(): return lax.ppermute(x, axis, [(i, (i + step) % size) for i in range(size)])  12.6 us
    pallas_call x7, Pallas kernels, call(): pl.pallas_call(kernel, out_shape=outs, in_specs=specs or [VM] * len(args)...  11.4 us
    all_to_all x1, waiting for transfers between devices, body(): lax.all_to_all(back.reshape(EXPERTS, BACK, LANES), ('z', 'x', 'c'), split...  9.88 us
    all_to_all x1, waiting for transfers between devices, body(): lax.all_to_all(hidden, 'y', split_axis=0, concat_axis=0, tiled=True)  5.36 us
    all_to_all x1, starting transfers between devices, body(): lax.all_to_all(hidden, 'y', split_axis=0, concat_axis=0, tiled=True)  3.87 us
  transfers between devices with their start and end apart: 14, of which 7 were waited for; matrix products, arithmetic and copies ran while one was open for 0% of the time, Pallas kernels for 1%

commit v1 on v0

--- a/solution.py
+++ b/solution.py
@@ -26,6 +26,8 @@
 NGROUPS = SLOTS // GROUP
 MSG = NC * FF_DEV + TOK
 ORDER = (0, 4, 5, 3, 6, 2, 7, 1)
+SENDS = 4
+LOADS = 3
 BATCH = 8
 PARTS = EP // BATCH
 BACK = 16
@@ -63,7 +65,19 @@
 
 
 def pack_kernel(
-    tok_hbm, gain_hbm, routes_hbm, send_ref, normed_ref, stack_ref, tok_ref, gain_ref, routes_ref, sems
+    tok_hbm,
+    gain_hbm,
+    routes_hbm,
+    send_hbm,
+    normed_hbm,
+    stack_ref,
+    tok_ref,
+    gain_ref,
+    routes_ref,
+    send_ref,
+    normed_ref,
+    sems,
+    out_sems,
 ):
     core = lax.axis_index("c")
     routes_copy = pltpu.make_async_copy(routes_hbm, routes_ref, sems.at[2])
@@ -72,16 +86,17 @@
     routes_copy.start()
     tok_copy.start()
     gain_copy.start()
-    routes_copy.wait()
-    code = spread_tokens(membership(routes_ref[...], CAP)).astype(BF16)
+    stack_ref[...] = jnp.zeros(stack_ref.shape, BF16)
     row, expert = iota((ROWS, EXPERTS), 0), iota((ROWS, EXPERTS), 1)
     low = (expert - core) * (PIECE // 2)
     owner = ((expert & 1) == core) & (row >= low) & (row < low + PIECE)
-    found = nn(owner.astype(F32).astype(BF16), code)
+    owner = owner.astype(F32).astype(BF16)
+    routes_copy.wait()
+    code = spread_tokens(membership(routes_ref[...], CAP)).astype(BF16)
+    found = nn(owner, code)
     row, col = iota((ROWS, LANES), 0), iota((ROWS, LANES), 1)
     table = (found == ((row >> 2) + 1).astype(F32)) & ((row & 3) == (col >> 5))
     table = table.astype(F32).astype(BF16)
-    stack_ref[...] = jnp.zeros(stack_ref.shape, BF16)
     tok_copy.wait()
     gain_copy.wait()
     values = tok_ref[...].astype(F32)
@@ -91,16 +106,32 @@
     normed_ref[...] = normed
     for q in range(QUARTERS):
         stack_ref[q * GROUP : q * GROUP + TOK, :] = normed[:, q * QW : (q + 1) * QW]
-    chunk = ROWS // 4
-    for k in range(4):
-        send_ref[k * chunk : (k + 1) * chunk, :] = nn(
-            table[k * chunk : (k + 1) * chunk, :], stack_ref[...]
-        ).astype(BF16)
-
-
-def side_kernel(normed_ref, sg_ref, su_ref, sd_ref, down_ref, *refs):
-    messages, part_ref = refs[:NY], refs[NY]
-    me = lax.axis_index("y")
+    chunk = ROWS // SENDS
+    copies = []
+    for k in range(SENDS):
+        rows = slice(k * chunk, (k + 1) * chunk)
+        send_ref[rows, :] = nn(table[rows, :], stack_ref[...]).astype(BF16)
+        copies.append(
+            pltpu.make_async_copy(send_ref.at[rows, :], send_hbm.at[rows, :], out_sems.at[k])
+        )
+        copies[k].start()
+    copies.append(pltpu.make_async_copy(normed_ref, normed_hbm, out_sems.at[SENDS]))
+    copies[SENDS].start()
+    for copy in copies:
+        copy.wait()
+
+
+def side_kernel(normed_ref, sg_ref, su_ref, sd_ref, down_ref, gate_hbm, up_hbm, *refs):
+    messages, (swap_ref, part_ref, sems) = refs[:NY], refs[NY:]
+    core, me = lax.axis_index("c"), lax.axis_index("y")
+    copies = [
+        pltpu.make_async_copy(
+            ref.at[1 - core], swap_ref.at[k * FF_DEV : (k + 1) * FF_DEV, :], sems.at[k]
+        )
+        for k, ref in enumerate((gate_hbm, up_hbm))
+    ]
+    for copy in copies:
+        copy.start()
     normed = normed_ref[...]
     gate, upper = nt(normed, sg_ref[...]), nt(normed, su_ref[...])
     hidden = (gate / (1.0 + jnp.exp(-gate)) * upper).astype(BF16)
@@ -110,11 +141,15 @@
         messages[d][0:FF_DEV, :] = down_ref[0, :, cols]
         messages[d][FF_DEV : 2 * FF_DEV, :] = down_ref[1, :, cols]
         messages[d][2 * FF_DEV : MSG, :] = part_ref[:, cols]
+    for copy in copies:
+        copy.wait()
 
 
 def ready_kernel(*refs):
-    messages, (keep_ref, give_ref, mine_ref, other_ref) = dict(zip(ORDER, refs)), refs[NY:]
+    messages = dict(zip(ORDER, refs))
+    keep_ref, give_ref, mine_ref, other_ref, flag_ref = refs[NY:]
     core, me = lax.axis_index("c"), lax.axis_index("y")
+    flag_ref[...] = jnp.zeros(flag_ref.shape, F32)
     shared = jnp.zeros((TOK, OUT_W), F32)
     for d in range(NY):
         source = lax.rem(me + NY - d, NY)
@@ -136,40 +171,35 @@
 
 
 def hidden_kernel(
-    rows_hbm,
-    gate_hbm,
-    got_gate_hbm,
-    up_hbm,
-    got_up_hbm,
-    after_ref,
-    out_ref,
-    rows_ref,
-    x_ref,
-    weight_ref,
-    row_sems,
-    sems,
+    rows_hbm, gate_hbm, up_hbm, got_hbm, flag_ref, out_ref, rows_ref, x_ref, weight_ref, row_sems, sems
 ):
     core = lax.axis_index("c")
+    size = ROWS // LOADS
     pieces = [
         pltpu.make_async_copy(
-            rows_hbm.at[g * LANES : (g + 1) * LANES, :],
-            rows_ref.at[g * LANES : (g + 1) * LANES, :],
-            row_sems.at[g],
+            rows_hbm.at[k * size : (k + 1) * size, :],
+            rows_ref.at[k * size : (k + 1) * size, :],
+            row_sems.at[k],
         )
-        for g in range(NGROUPS)
+        for k in range(LOADS)
     ]
+    sources = (
+        gate_hbm.at[core],
+        got_hbm.at[0:FF_DEV],
+        up_hbm.at[core],
+        got_hbm.at[FF_DEV : 2 * FF_DEV],
+    )
     copies = [
-        pltpu.make_async_copy(
-            ref.at[core], weight_ref.at[k * FF_DEV : (k + 1) * FF_DEV, :], sems.at[k]
-        )
-        for k, ref in enumerate((gate_hbm, got_gate_hbm, up_hbm, got_up_hbm))
+        pltpu.make_async_copy(ref, weight_ref.at[k * FF_DEV : (k + 1) * FF_DEV, :], sems.at[k])
+        for k, ref in enumerate(sources)
     ]
     for copy in pieces + copies:
         copy.start()
     i, j = iota((LANES, LANES), 0), iota((LANES, LANES), 1)
     sort = (j == (i & (GROUP - 1)) * QUARTERS + (i >> 5)).astype(F32).astype(BF16)
     for g in range(NGROUPS):
-        pieces[g].wait()
+        if g * LANES % size == 0:
+            pieces[g * LANES // size].wait()
         block = nn(sort, rows_ref[g * LANES : (g + 1) * LANES, :]).astype(BF16)
         for q in range(QUARTERS):
             x_ref[g * GROUP : (g + 1) * GROUP, q * QW : (q + 1) * QW] = block[
@@ -241,12 +271,12 @@
         ).astype(BF16)
 
 
-def call(kernel, outs, scratch, flops, *args, specs=None, grant=24):
+def call(kernel, outs, scratch, flops, *args, specs=None, out_specs=None, grant=24):
     return pl.pallas_call(
         kernel,
         out_shape=outs,
         in_specs=specs or [VM] * len(args),
-        out_specs=jax.tree.map(lambda _: VM, outs),
+        out_specs=out_specs or jax.tree.map(lambda _: VM, outs),
         scratch_shapes=scratch,
         compiler_params=pltpu.CompilerParams(vmem_limit_bytes=grant << 20),
         cost_estimate=pl.CostEstimate(flops=flops, bytes_accessed=1 << 20, transcendentals=0),
@@ -281,35 +311,39 @@
             pltpu.VMEM((TOK, D), BF16),
             pltpu.VMEM((1, D), F32),
             pltpu.VMEM((TOPK, TOK), jnp.int32),
+            pltpu.VMEM((ROWS, QW), BF16),
+            pltpu.VMEM((TOK, D), BF16),
             pltpu.SemaphoreType.DMA((3,)),
+            pltpu.SemaphoreType.DMA((SENDS + 1,)),
         ],
         1 << 30,
         tokens,
         norm_gain.reshape(1, D),
         routes.T,
         specs=[HB] * 3,
+        out_specs=(HB, HB),
         grant=62,
     )
     rows = lax.all_to_all(
         send.reshape(EP, PIECE, QW), ("z", "x"), split_axis=0, concat_axis=0, tiled=True
     ).reshape(ROWS, QW)
-    messages = list(
-        call(
-            side_kernel,
-            tuple(out((MSG, OUT_W)) for _ in range(NY)),
-            [pltpu.VMEM((TOK, D), BF16)],
-            1 << 30,
-            normed,
-            shared_gate,
-            shared_up,
-            shared_down,
-            expert_down,
-        )
+    *messages, swap = call(
+        side_kernel,
+        tuple(out((MSG, OUT_W)) for _ in range(NY)) + (out((2 * FF_DEV, D)),),
+        [pltpu.VMEM((TOK, D), BF16), pltpu.SemaphoreType.DMA((2,))],
+        1 << 30,
+        normed,
+        shared_gate,
+        shared_up,
+        shared_down,
+        expert_down,
+        expert_gate,
+        expert_up,
+        specs=[VM] * 5 + [HB] * 2,
     )
     for d in ORDER[1:]:
         messages[d] = hop(messages[d], "y", NY, d)
-    got_gate = hop(expert_gate, "c", NC, 1)
-    got_up = hop(expert_up, "c", NC, 1)
+    swapped = hop(swap, "c", NC, 1)
     chi, clo = call(
         weigh_kernel,
         (out((NC * GROUP, BACK_ROWS)), out((NC * GROUP, BACK_ROWS))),
@@ -319,9 +353,15 @@
         route_scores.T,
     )
     wide = NY * FF_DEV
-    keep, give, mine, other = call(
+    keep, give, mine, other, flag = call(
         ready_kernel,
-        (out((wide, OUT_W)), out((wide, OUT_W)), out((TOK, HALF), F32), out((TOK, HALF), F32)),
+        (
+            out((wide, OUT_W)),
+            out((wide, OUT_W)),
+            out((TOK, HALF), F32),
+            out((TOK, HALF), F32),
+            out((8, LANES), F32),
+        ),
         [],
         1 << 28,
         *[messages[d] for d in ORDER],
@@ -334,18 +374,17 @@
             pltpu.VMEM((ROWS, QW), BF16),
             pltpu.VMEM((SLOTS, D), BF16),
             pltpu.VMEM((4 * FF_DEV, D), BF16),
-            pltpu.SemaphoreType.DMA((NGROUPS,)),
+            pltpu.SemaphoreType.DMA((LOADS,)),
             pltpu.SemaphoreType.DMA((4,)),
         ],
         1 << 30,
         rows,
         expert_gate,
-        got_gate,
         expert_up,
-        got_up,
-        mine,
-        specs=[HB] * 5 + [VM],
-        grant=60,
+        swapped,
+        flag,
+        specs=[HB] * 4 + [VM],
+        grant=52,
     )
     hidden = lax.all_to_all(hidden, "y", split_axis=0, concat_axis=0, tiled=True)
     back = call(

time: 115 us -> 114 us (level)
  local copies, waits for them, and re-layouts: 0.63 us -> 5.01 us
  waiting for transfers between devices: 27.8 us -> 23.6 us
    unnamed x18 -> x20, local copies, waits for them, and re-layouts: 0.63 us -> 5.01 us
    all_to_all x1, waiting for transfers between devices: 5.36 us -> 1.67 us  [body(): lax.all_to_all(hidden, 'y', split_axis=0, concat_axis=0, tiled=True)]
    ppermute x11 -> x10, starting transfers between devices: 42 us -> 39.5 us  [hop(): return lax.ppermute(x, axis, [(i, (i + step) % size) for i in range(size)])]
    all_to_all x1, starting transfers between devices: 14.5 us -> 16.6 us  [body(): lax.all_to_all(back.reshape(EXPERTS, BACK, LANES), ('z', 'x', 'c'), split...]
    pallas_call x7, Pallas kernels: 11.4 us -> 10.3 us  [call(): pl.pallas_call(kernel, out_shape=outs, in_specs=specs or [VM] * len(args)...]
    ppermute x11 -> x10, waiting for transfers between devices: 12.6 us -> 12.1 us  [hop(): return lax.ppermute(x, axis, [(i, (i + step) % size) for i in range(size)])]
  transfers between devices with their start and end apart: 14 -> 13, of which waited for: 7 -> 8; matrix products, arithmetic and copies ran while one was open for 0% -> 0% of each run, Pallas kernels for 1% -> 1%
where the time goes in v1:
time: 114 us; the launch traced here: 113 us
  starting transfers between devices  73.6 us (65%)
  waiting for transfers between devices  23.6 us (21%)
  Pallas kernels  10.3 us (9%)
  local copies, waits for them, and re-layouts  5.01 us (4%)
    ppermute x10, starting transfers between devices, hop(): return lax.ppermute(x, axis, [(i, (i + step) % size) for i in range(size)])  39.5 us
    all_to_all x1, starting transfers between devices, body(): lax.all_to_all(back.reshape(EXPERTS, BACK, LANES), ('z', 'x', 'c'), split...  16.6 us
    all_to_all x1, starting transfers between devices, body(): lax.all_to_all(send.reshape(EP, PIECE, QW), ('z', 'x'), split_axis=0, con...  14.1 us
    ppermute x10, waiting for transfers between devices, hop(): return lax.ppermute(x, axis, [(i, (i + step) % size) for i in range(size)])  12.1 us
    pallas_call x7, Pallas kernels, call(): pl.pallas_call(kernel, out_shape=outs, in_specs=specs or [VM] * len(args)...  10.3 us
    all_to_all x1, waiting for transfers between devices, body(): lax.all_to_all(back.reshape(EXPERTS, BACK, LANES), ('z', 'x', 'c'), split...  9.88 us
    unnamed x20, local copies, waits for them, and re-layouts  5.01 us
    all_to_all x1, starting transfers between devices, body(): lax.all_to_all(hidden, 'y', split_axis=0, concat_axis=0, tiled=True)  3.52 us
  transfers between devices with their start and end apart: 13, of which 8 were waited for; matrix products, arithmetic and copies ran while one was open for 0% of the time, Pallas kernels for 1%

profile of v1, /device:TPU:1, one launch (start us, length us, event | category | flops | bytes accessed | tf_op | source)
XLA Modules:
  0.0 112.8 jit_solution(4791321810547572775)
XLA Ops:
  0.0 2.9 %shard_map.100 = (bf16[768,1024]{1,0:T(8,128)(2,1)}, bf16[24,4096]{1,0:T(8,128)(2,1)}) custom-call(bf16[24,4096]{1,0:T(8,128)(2,1)} %tok_hbm.1, f32[1,4096]{1,0:T(1,128)} %bitcast.12, s32[6,24]{1,0:T(8,128)} %bitcast.8), custom_call_target="tpu_custom_call" | custom-call | flops 1073741824 | bytes 1048576 | tf_op jit(solution)/shard_map/pallas_call | solution.py:275
  2.9 0.0 copy-start
  2.9 0.0 copy-start.1
  3.0 0.0 copy-start.2
  3.0 14.1 %all-to-all-start = ((bf16[32,24,1024]{2,1,0:T(8,128)(2,1)}), bf16[32,24,1024]{2,1,0:T(8,128)(2,1)}, u32[]{:S(2)}, u32[]{:S(2)}) async-start(bf16[32,24,1024]{2,1,0:T(8,128)(2,1)} %bitcast.11), calls=%async_computation | async-start | bytes 3145728 | tf_op jit(solution)/shard_map/all_to_all | solution.py:327
  17.1 0.0 copy-done
  17.1 0.0 copy-done.1
  17.1 0.0 copy-done.2
  17.1 0.0 copy-start.3
  17.1 1.0 copy-done.3
  18.1 1.0 copy-done.4
  19.2 1.0 copy-done.5
  20.2 0.9 copy-done.6
  21.2 0.7 shard_map.101
  21.9 2.9 %collective-permute-start = (bf16[128,4096]{1,0:T(8,128)(2,1)S(1)}, bf16[128,4096]{1,0:T(8,128)(2,1)S(1)}, u32[]{:S(2)}, u32[]{:S(2)}) collective-permute-start(bf16[128,4096]{1,0:T(8,128)(2,1)S(1)} %get-tuple-element.25), channel_id=1, source_target_pairs={{0,1},{1,0},{2,3},{3,2},{4,5},{5,4},{6,7},{7,6},{8,9},{9,8},{10,11... | collective-permute-start | bytes 3145736 | tf_op jit(solution)/shard_map/ppermute | solution.py:291
  24.8 7.5 %collective-permute-start.1 = (bf16[152,512]{1,0:T(8,128)(2,1)S(1)}, bf16[152,512]{1,0:T(8,128)(2,1)S(1)}, u32[]{:S(2)}, u32[]{:S(2)}) collective-permute-start(bf16[152,512]{1,0:T(8,128)(2,1)S(1)} %get-tuple-element.27), channel_id=1, source_target_pairs={{0,8},{2,10},{4,12},{6,14},{8,0},{10,2},{12,4},{14,6},{1,9},{3,11}... | collective-permute-start | bytes 466952 | tf_op jit(solution)/shard_map/ppermute | solution.py:291
  32.2 1.9 %collective-permute-start.2 = (bf16[152,512]{1,0:T(8,128)(2,1)S(1)}, bf16[152,512]{1,0:T(8,128)(2,1)S(1)}, u32[]{:S(2)}, u32[]{:S(2)}) collective-permute-start(bf16[152,512]{1,0:T(8,128)(2,1)S(1)} %get-tuple-element.28), channel_id=1, source_target_pairs={{0,10},{2,12},{4,14},{6,0},{8,2},{10,4},{12,6},{14,8},{1,11},{3,13... | collective-permute-start | bytes 466952 | tf_op jit(solution)/shard_map/ppermute | solution.py:291
  34.2 5.2 %collective-permute-start.3 = (bf16[152,512]{1,0:T(8,128)(2,1)S(1)}, bf16[152,512]{1,0:T(8,128)(2,1)S(1)}, u32[]{:S(2)}, u32[]{:S(2)}) collective-permute-start(bf16[152,512]{1,0:T(8,128)(2,1)S(1)} %get-tuple-element.29), channel_id=1, source_target_pairs={{0,6},{2,8},{4,10},{6,12},{8,14},{10,0},{12,2},{14,4},{1,7},{3,9},... | collective-permute-start | bytes 466952 | tf_op jit(solution)/shard_map/ppermute | solution.py:291
  39.3 3.2 %collective-permute-start.4 = (bf16[152,512]{1,0:T(8,128)(2,1)S(1)}, bf16[152,512]{1,0:T(8,128)(2,1)S(1)}, u32[]{:S(2)}, u32[]{:S(2)}) collective-permute-start(bf16[152,512]{1,0:T(8,128)(2,1)S(1)} %get-tuple-element.30), channel_id=1, source_target_pairs={{0,12},{2,14},{4,0},{6,2},{8,4},{10,6},{12,8},{14,10},{1,13},{3,15... | collective-permute-start | bytes 466952 | tf_op jit(solution)/shard_map/ppermute | solution.py:291
  42.5 0.0 collective-permute-done.1.refs_1_
  42.5 3.0 %collective-permute-start.5 = (bf16[152,512]{1,0:T(8,128)(2,1)S(1)}, bf16[152,512]{1,0:T(8,128)(2,1)S(1)}, u32[]{:S(2)}, u32[]{:S(2)}) collective-permute-start(bf16[152,512]{1,0:T(8,128)(2,1)S(1)} %get-tuple-element.31), channel_id=1, source_target_pairs={{0,4},{2,6},{4,8},{6,10},{8,12},{10,14},{12,0},{14,2},{1,5},{3,7},... | collective-permute-start | bytes 466952 | tf_op jit(solution)/shard_map/ppermute | solution.py:291
  45.5 5.1 %collective-permute-done.2.refs_2_ = bf16[152,512]{1,0:T(8,128)(2,1)S(1)} collective-permute-done((bf16[152,512]{1,0:T(8,128)(2,1)S(1)}, bf16[152,512]{1,0:T(8,128)(2,1)S(1)}, u32[]{:S(2)}, u32[]{:S(2)}) %collective-permute-start.2) | collective-permute-done | bytes 155680 | tf_op jit(solution)/shard_map/ppermute | solution.py:291
  50.6 3.9 %collective-permute-start.6 = (bf16[152,512]{1,0:T(8,128)(2,1)S(1)}, bf16[152,512]{1,0:T(8,128)(2,1)S(1)}, u32[]{:S(2)}, u32[]{:S(2)}) collective-permute-start(bf16[152,512]{1,0:T(8,128)(2,1)S(1)} %get-tuple-element.32), channel_id=1, source_target_pairs={{0,14},{2,0},{4,2},{6,4},{8,6},{10,8},{12,10},{14,12},{1,15},{3,1}... | collective-permute-start | bytes 466952 | tf_op jit(solution)/shard_map/ppermute | solution.py:291
  54.6 0.0 collective-permute-done.3.refs_3_
  54.6 1.9 %collective-permute-start.7 = (bf16[152,512]{1,0:T(8,128)(2,1)S(1)}, bf16[152,512]{1,0:T(8,128)(2,1)S(1)}, u32[]{:S(2)}, u32[]{:S(2)}) collective-permute-start(bf16[152,512]{1,0:T(8,128)(2,1)S(1)} %get-tuple-element.33), channel_id=1, source_target_pairs={{0,2},{2,4},{4,6},{6,8},{8,10},{10,12},{12,14},{14,0},{1,3},{3,5},... | collective-permute-start | bytes 466952 | tf_op jit(solution)/shard_map/ppermute | solution.py:291
  56.5 1.0 collective-permute-done.4.refs_4_
  57.5 0.0 collective-permute-done.5.refs_5_
  57.5 2.5 %collective-permute-done.6.refs_6_ = bf16[152,512]{1,0:T(8,128)(2,1)S(1)} collective-permute-done((bf16[152,512]{1,0:T(8,128)(2,1)S(1)}, bf16[152,512]{1,0:T(8,128)(2,1)S(1)}, u32[]{:S(2)}, u32[]{:S(2)}) %collective-permute-start.6) | collective-permute-done | bytes 155680 | tf_op jit(solution)/shard_map/ppermute | solution.py:291
  60.0 1.7 %collective-permute-done.7.refs_7_ = bf16[152,512]{1,0:T(8,128)(2,1)S(1)} collective-permute-done((bf16[152,512]{1,0:T(8,128)(2,1)S(1)}, bf16[152,512]{1,0:T(8,128)(2,1)S(1)}, u32[]{:S(2)}, u32[]{:S(2)}) %collective-permute-start.7) | collective-permute-done | bytes 155680 | tf_op jit(solution)/shard_map/ppermute | solution.py:291
  61.8 0.1 shard_map.102
  61.9 0.0 collective-permute-done.got_hbm
  61.9 0.0 copy-start.9
  61.9 0.0 all-to-all-done
  61.9 0.9 copy-done.9
  62.9 3.6 %shard_map.103 = bf16[8,192,128]{2,1,0:T(8,128)(2,1)} custom-call(bf16[768,1024]{1,0:T(8,128)(2,1)} %bitcast.3.rows_hbm, bf16[2,64,4096]{2,1,0:T(8,128)(2,1)S(1)} %copy-done, bf16[2,64,4096]{2,1,0:T(8,128)(2,1)} %up_hbm.3, bf16[128,4096]{1,0:T(8,128)(2,1)} %copy-done.9, f32[8,128]{1,0:T(8,128)S(1)} %get-tuple-element.34.flag_ref), custom_call_target="tpu_custom_call" | custom-call | flops 1073741824 | bytes 1048576 | tf_op jit(solution)/shard_map/pallas_call | solution.py:275
  66.5 3.5 %all-to-all-start.1 = ((bf16[8,192,128]{2,1,0:T(8,128)(2,1)}), bf16[8,192,128]{2,1,0:T(8,128)(2,1)S(1)}, u32[]{:S(2)}, u32[]{:S(2)}) async-start(bf16[8,192,128]{2,1,0:T(8,128)(2,1)} %shard_map.103), calls=%async_computation.1 | async-start | bytes 786432 | tf_op jit(solution)/shard_map/all_to_all | solution.py:389
  70.0 7.7 %collective-permute-start.8 = (bf16[512,512]{1,0:T(8,128)(2,1)S(1)}, bf16[512,512]{1,0:T(8,128)(2,1)S(1)}, u32[]{:S(2)}, u32[]{:S(2)}) collective-permute-start(bf16[512,512]{1,0:T(8,128)(2,1)S(1)} %get-tuple-element.36), channel_id=1, source_target_pairs={{0,1},{1,0},{2,3},{3,2},{4,5},{5,4},{6,7},{7,6},{8,9},{9,8},{10,11... | collective-permute-start | bytes 1572872 | tf_op jit(solution)/shard_map/ppermute | solution.py:291
  77.7 1.5 %collective-permute-done.8.got_ref = bf16[512,512]{1,0:T(8,128)(2,1)S(1)} collective-permute-done((bf16[512,512]{1,0:T(8,128)(2,1)S(1)}, bf16[512,512]{1,0:T(8,128)(2,1)S(1)}, u32[]{:S(2)}, u32[]{:S(2)}) %collective-permute-start.8) | collective-permute-done | bytes 524320 | tf_op jit(solution)/shard_map/ppermute | solution.py:291
  79.2 1.7 %all-to-all-done.1.hidden_ref = bf16[8,192,128]{2,1,0:T(8,128)(2,1)S(1)} async-done(((bf16[8,192,128]{2,1,0:T(8,128)(2,1)}), bf16[8,192,128]{2,1,0:T(8,128)(2,1)S(1)}, u32[]{:S(2)}, u32[]{:S(2)}) %all-to-all-start.1) | async-done | bytes 393248 | tf_op jit(solution)/shard_map/all_to_all | solution.py:389
  80.9 1.5 %shard_map.104 = bf16[1024,128]{1,0:T(8,128)(2,1)} custom-call(bf16[8,192,128]{2,1,0:T(8,128)(2,1)S(1)} %all-to-all-done.1.hidden_ref, bf16[512,512]{1,0:T(8,128)(2,1)S(1)} %get-tuple-element.35.keep_ref, bf16[512,512]{1,0:T(8,128)(2,1)S(1)} %collective-permute-done.8.got_ref), custom_call_target="tpu_custom_call" | custom-call | flops 1073741824 | bytes 1048576 | tf_op jit(solution)/shard_map/pallas_call | solution.py:275
  82.3 16.6 %all-to-all-start.2 = ((bf16[64,16,128]{2,1,0:T(8,128)(2,1)}), bf16[64,16,128]{2,1,0:T(8,128)(2,1)S(1)}, u32[]{:S(2)}, u32[]{:S(2)}) async-start(bf16[64,16,128]{2,1,0:T(8,128)(2,1)} %bitcast.4), calls=%async_computation.2 | async-start | bytes 524288 | tf_op jit(solution)/shard_map/all_to_all | solution.py:399
  98.9 2.4 %collective-permute-start.9 = (f32[24,256]{1,0:T(8,128)S(1)}, f32[24,256]{1,0:T(8,128)S(1)}, u32[]{:S(2)}, u32[]{:S(2)}) collective-permute-start(f32[24,256]{1,0:T(8,128)S(1)} %get-tuple-element.40), channel_id=1, source_target_pairs={{0,1},{1,0},{2,3},{3,2},{4,5},{5,4},{6,7},{7,6},{8,9},{9,8},{10,11... | collective-permute-start | bytes 73736 | tf_op jit(solution)/shard_map/ppermute | solution.py:291
  101.3 0.0 copy-done.7
  101.3 0.0 copy-done.8
  101.3 0.6 shard_map.105
  101.9 0.2 collective-permute-done.9.got_ref
  102.1 9.9 %all-to-all-done.2 = bf16[64,16,128]{2,1,0:T(8,128)(2,1)S(1)} async-done(((bf16[64,16,128]{2,1,0:T(8,128)(2,1)}), bf16[64,16,128]{2,1,0:T(8,128)(2,1)S(1)}, u32[]{:S(2)}, u32[]{:S(2)}) %all-to-all-start.2) | async-done | bytes 262176 | tf_op jit(solution)/shard_map/all_to_all | solution.py:399
  112.0 0.8 shard_map.106
  (5 shorter events, 0.0 us)
Async XLA Ops:
  2.9 14.1 %copy-start = (bf16[2,64,4096]{2,1,0:T(8,128)(2,1)S(1)}, bf16[2,64,4096]{2,1,0:T(8,128)(2,1)}, u32[]{:S(2)}) copy-start(bf16[2,64,4096]{2,1,0:T(8,128)(2,1)} %gate_hbm.3) | copy-start | bytes 3145732
  2.9 14.1 %copy-start.1 = (bf16[2,64,4096]{2,1,0:T(8,128)(2,1)S(1)}, bf16[2,64,4096]{2,1,0:T(8,128)(2,1)}, u32[]{:S(2)}) copy-start(bf16[2,64,4096]{2,1,0:T(8,128)(2,1)} %up_hbm.3) | copy-start | bytes 3145732
  3.0 14.1 %copy-start.2 = (bf16[2,64,4096]{2,1,0:T(8,128)(2,1)S(1)}, bf16[2,64,4096]{2,1,0:T(8,128)(2,1)}, u32[]{:S(2)}) copy-start(bf16[2,64,4096]{2,1,0:T(8,128)(2,1)} %down_ref.1) | copy-start | bytes 3145732
  3.0 59.0 %all-to-all-start = ((bf16[32,24,1024]{2,1,0:T(8,128)(2,1)}), bf16[32,24,1024]{2,1,0:T(8,128)(2,1)}, u32[]{:S(2)}, u32[]{:S(2)}) async-start(bf16[32,24,1024]{2,1,0:T(8,128)(2,1)} %bitcast.11), calls=%async_computation | async-start | bytes 3145728 | tf_op jit(solution)/shard_map/all_to_all | solution.py:327
  17.1 1.0 copy-start.3
  18.1 1.0 copy-start.4
  19.2 1.0 copy-start.5
  20.2 0.9 copy-start.6
  21.9 40.0 %collective-permute-start = (bf16[128,4096]{1,0:T(8,128)(2,1)S(1)}, bf16[128,4096]{1,0:T(8,128)(2,1)S(1)}, u32[]{:S(2)}, u32[]{:S(2)}) collective-permute-start(bf16[128,4096]{1,0:T(8,128)(2,1)S(1)} %get-tuple-element.25), channel_id=1, source_target_pairs={{0,1},{1,0},{2,3},{3,2},{4,5},{5,4},{6,7},{7,6},{8,9},{9,8},{10,11... | collective-permute-start | bytes 3145736 | tf_op jit(solution)/shard_map/ppermute | solution.py:291
  24.8 17.7 %collective-permute-start.1 = (bf16[152,512]{1,0:T(8,128)(2,1)S(1)}, bf16[152,512]{1,0:T(8,128)(2,1)S(1)}, u32[]{:S(2)}, u32[]{:S(2)}) collective-permute-start(bf16[152,512]{1,0:T(8,128)(2,1)S(1)} %get-tuple-element.27), channel_id=1, source_target_pairs={{0,8},{2,10},{4,12},{6,14},{8,0},{10,2},{12,4},{14,6},{1,9},{3,11}... | collective-permute-start | bytes 466952 | tf_op jit(solution)/shard_map/ppermute | solution.py:291
  32.2 18.4 %collective-permute-start.2 = (bf16[152,512]{1,0:T(8,128)(2,1)S(1)}, bf16[152,512]{1,0:T(8,128)(2,1)S(1)}, u32[]{:S(2)}, u32[]{:S(2)}) collective-permute-start(bf16[152,512]{1,0:T(8,128)(2,1)S(1)} %get-tuple-element.28), channel_id=1, source_target_pairs={{0,10},{2,12},{4,14},{6,0},{8,2},{10,4},{12,6},{14,8},{1,11},{3,13... | collective-permute-start | bytes 466952 | tf_op jit(solution)/shard_map/ppermute | solution.py:291
  34.2 20.4 %collective-permute-start.3 = (bf16[152,512]{1,0:T(8,128)(2,1)S(1)}, bf16[152,512]{1,0:T(8,128)(2,1)S(1)}, u32[]{:S(2)}, u32[]{:S(2)}) collective-permute-start(bf16[152,512]{1,0:T(8,128)(2,1)S(1)} %get-tuple-element.29), channel_id=1, source_target_pairs={{0,6},{2,8},{4,10},{6,12},{8,14},{10,0},{12,2},{14,4},{1,7},{3,9},... | collective-permute-start | bytes 466952 | tf_op jit(solution)/shard_map/ppermute | solution.py:291
  39.3 18.2 %collective-permute-start.4 = (bf16[152,512]{1,0:T(8,128)(2,1)S(1)}, bf16[152,512]{1,0:T(8,128)(2,1)S(1)}, u32[]{:S(2)}, u32[]{:S(2)}) collective-permute-start(bf16[152,512]{1,0:T(8,128)(2,1)S(1)} %get-tuple-element.30), channel_id=1, source_target_pairs={{0,12},{2,14},{4,0},{6,2},{8,4},{10,6},{12,8},{14,10},{1,13},{3,15... | collective-permute-start | bytes 466952 | tf_op jit(solution)/shard_map/ppermute | solution.py:291
  42.5 15.0 %collective-permute-start.5 = (bf16[152,512]{1,0:T(8,128)(2,1)S(1)}, bf16[152,512]{1,0:T(8,128)(2,1)S(1)}, u32[]{:S(2)}, u32[]{:S(2)}) collective-permute-start(bf16[152,512]{1,0:T(8,128)(2,1)S(1)} %get-tuple-element.31), channel_id=1, source_target_pairs={{0,4},{2,6},{4,8},{6,10},{8,12},{10,14},{12,0},{14,2},{1,5},{3,7},... | collective-permute-start | bytes 466952 | tf_op jit(solution)/shard_map/ppermute | solution.py:291
  50.6 9.4 %collective-permute-start.6 = (bf16[152,512]{1,0:T(8,128)(2,1)S(1)}, bf16[152,512]{1,0:T(8,128)(2,1)S(1)}, u32[]{:S(2)}, u32[]{:S(2)}) collective-permute-start(bf16[152,512]{1,0:T(8,128)(2,1)S(1)} %get-tuple-element.32), channel_id=1, source_target_pairs={{0,14},{2,0},{4,2},{6,4},{8,6},{10,8},{12,10},{14,12},{1,15},{3,1}... | collective-permute-start | bytes 466952 | tf_op jit(solution)/shard_map/ppermute | solution.py:291
  54.6 7.2 %collective-permute-start.7 = (bf16[152,512]{1,0:T(8,128)(2,1)S(1)}, bf16[152,512]{1,0:T(8,128)(2,1)S(1)}, u32[]{:S(2)}, u32[]{:S(2)}) collective-permute-start(bf16[152,512]{1,0:T(8,128)(2,1)S(1)} %get-tuple-element.33), channel_id=1, source_target_pairs={{0,2},{2,4},{4,6},{6,8},{8,10},{10,12},{12,14},{14,0},{1,3},{3,5},... | collective-permute-start | bytes 466952 | tf_op jit(solution)/shard_map/ppermute | solution.py:291
  61.9 1.0 copy-start.9
  66.5 14.4 %all-to-all-start.1 = ((bf16[8,192,128]{2,1,0:T(8,128)(2,1)}), bf16[8,192,128]{2,1,0:T(8,128)(2,1)S(1)}, u32[]{:S(2)}, u32[]{:S(2)}) async-start(bf16[8,192,128]{2,1,0:T(8,128)(2,1)} %shard_map.103), calls=%async_computation.1 | async-start | bytes 786432 | tf_op jit(solution)/shard_map/all_to_all | solution.py:389
  70.0 9.2 %collective-permute-start.8 = (bf16[512,512]{1,0:T(8,128)(2,1)S(1)}, bf16[512,512]{1,0:T(8,128)(2,1)S(1)}, u32[]{:S(2)}, u32[]{:S(2)}) collective-permute-start(bf16[512,512]{1,0:T(8,128)(2,1)S(1)} %get-tuple-element.36), channel_id=1, source_target_pairs={{0,1},{1,0},{2,3},{3,2},{4,5},{5,4},{6,7},{7,6},{8,9},{9,8},{10,11... | collective-permute-start | bytes 1572872 | tf_op jit(solution)/shard_map/ppermute | solution.py:291
  80.9 20.4 %copy-start.7 = (s32[24,6]{0,1:T(8,128)S(1)}, s32[24,6]{0,1:T(8,128)}, u32[]{:S(2)}) copy-start(s32[24,6]{0,1:T(8,128)} %param.12) | copy-start | bytes 1732
  80.9 20.4 %copy-start.8 = (f32[24,6]{0,1:T(8,128)S(1)}, f32[24,6]{0,1:T(8,128)}, u32[]{:S(2)}) copy-start(f32[24,6]{0,1:T(8,128)} %param.13) | copy-start | bytes 1732
  82.3 29.7 %all-to-all-start.2 = ((bf16[64,16,128]{2,1,0:T(8,128)(2,1)}), bf16[64,16,128]{2,1,0:T(8,128)(2,1)S(1)}, u32[]{:S(2)}, u32[]{:S(2)}) async-start(bf16[64,16,128]{2,1,0:T(8,128)(2,1)} %bitcast.4), calls=%async_computation.2 | async-start | bytes 524288 | tf_op jit(solution)/shard_map/all_to_all | solution.py:399
  98.9 3.2 %collective-permute-start.9 = (f32[24,256]{1,0:T(8,128)S(1)}, f32[24,256]{1,0:T(8,128)S(1)}, u32[]{:S(2)}, u32[]{:S(2)}) collective-permute-start(f32[24,256]{1,0:T(8,128)S(1)} %get-tuple-element.40), channel_id=1, source_target_pairs={{0,1},{1,0},{2,3},{3,2},{4,5},{5,4},{6,7},{7,6},{8,9},{9,8},{10,11... | collective-permute-start | bytes 73736 | tf_op jit(solution)/shard_map/ppermute | solution.py:291
